TPU v7x, 32 devices: a whole 2x2x4 slice. The times are simulated.
32 devices in a mesh: sp: 8 (over z, y), tp: 4 (over x, core).
Axes of the slice: x: 2, y: 2, z: 4, core: 2. Of those that a mesh axis runs over, the one named last changes fastest.
Arguments:
- resid: bfloat16 [4096, 2048], P('sp', 'tp'), may hold values from -41 to 41
- queries: bfloat16 [4096, 1024], P('sp', 'tp'), may hold values from -6 to 6
- keys: bfloat16 [4096, 1024], P('sp', 'tp'), may hold values from -6 to 6
- values: bfloat16 [4096, 1024], P('sp', 'tp'), may hold values from -6 to 6
- mix_lambda: float32 [8], P('tp'), may hold values from 0.3 to 0.8
- head_gain: float32 [128], replicated, may hold values from 0.1 to 1.9
- out_weight: bfloat16 [1024, 2048], P(None, 'tp'), may hold values from -0.1875 to 0.1875
- norm_gain: float32 [2048], P('tp'), may hold values from 0.1 to 1.9
- gate_weight: bfloat16 [2048, 5632], P('sp', 'tp'), may hold values from -0.125 to 0.125
- up_weight: bfloat16 [2048, 5632], P('sp', 'tp'), may hold values from -0.125 to 0.125
- conv_weight: float32 [3, 5632], P(None, 'tp'), may hold values from -3.5 to 3.5
- conv_bias: float32 [5632], P('tp'), may hold values from -3 to 3
- down_weight: bfloat16 [5632, 2048], P('tp', 'sp'), may hold values from -0.078125 to 0.078125
Outputs:
- layer_out: bfloat16 [4096, 2048], P('sp', 'tp')
All inputs are finite; a program needn't handle non-finite values.
Results may differ from a plain program's by a relative error of at most 0.009.
Values may be sent and summed in bfloat16 or wider, within the bound.
A program may use at most 128 MiB of HBM per device.

v0:
```python
import math
import jax
import jax.numpy as jnp
from jax import lax
from jax.sharding import PartitionSpec as P

D = 2048
HD = 64
VD = 128


def with_halo(cells, sides, width):
    for axis, dim in sides:
        count = lax.axis_size(axis)
        ends = count - 1
        head = lax.slice_in_dim(cells, 0, width, axis=dim)
        tail = lax.slice_in_dim(cells, cells.shape[dim] - width, cells.shape[dim], axis=dim)
        cells = jnp.concatenate(
            [
                lax.ppermute(tail, axis, [(i, (i + 1) % count) for i in range(ends)]),
                cells,
                lax.ppermute(head, axis, [((i + 1) % count, i) for i in range(ends)]),
            ],
            axis=dim,
        )
    return cells


def on_device(
    resid,
    queries,
    keys,
    values,
    mix_lambda,
    head_gain,
    out_weight,
    norm_gain,
    gate_weight,
    up_weight,
    conv_weight,
    conv_bias,
    down_weight,
):
    length = queries.shape[0]
    heads = mix_lambda.shape[0]
    scale = HD ** (-0.5)
    query_heads = queries.reshape(length, heads, 2, HD)
    initial = (
        jnp.full((heads, 2, length), -1e30, jnp.float32),
        jnp.zeros((heads, 2, length), jnp.float32),
        jnp.zeros((heads, 2, length, VD), jnp.float32),
    )
    key_rows = lax.all_gather(keys, "sp", axis=0, tiled=True)
    value_rows = lax.all_gather(values, "sp", axis=0, tiled=True)
    count = key_rows.shape[0]
    block = math.gcd(count, 2048)
    key_blocks = key_rows.reshape(count // block, block, heads, 2, HD)
    value_blocks = value_rows.reshape(count // block, block, heads, VD)

    def advance(state, blocks):
        running, totals, weighted = state
        key_block, value_block = blocks
        scores = (
            jnp.einsum(
                "qhmd,khmd->hmqk", query_heads, key_block, preferred_element_type=jnp.float32
            )
            * scale
        )
        highest = jnp.maximum(running, jnp.max(scores, axis=-1))
        factor = jnp.exp(running - highest)
        shifted = jnp.exp(scores - highest[..., None])
        totals = totals * factor + jnp.sum(shifted, axis=-1)
        weighted = weighted * factor[..., None] + jnp.einsum(
            "hmqk,khe->hmqe",
            shifted.astype(jnp.bfloat16),
            value_block,
            preferred_element_type=jnp.float32,
        )
        return ((highest, totals, weighted), None)

    result, unused = lax.scan(advance, initial, (key_blocks, value_blocks))
    running, totals, weighted = result
    mapped = weighted / totals[..., None]
    mixed = mapped[:, 0] - mix_lambda[:, None, None] * mapped[:, 1]
    spread = jnp.mean(mixed * mixed, axis=-1, keepdims=True)
    normed = mixed * lax.rsqrt(spread + 1e-06) * head_gain * 0.8
    heads_out = jnp.transpose(normed, (1, 0, 2)).reshape(length, heads * VD).astype(jnp.bfloat16)
    projected = jnp.dot(
        lax.all_gather(heads_out, "tp", axis=1, tiled=True),
        out_weight,
        preferred_element_type=jnp.float32,
    )
    after_mixer = resid.astype(jnp.float32) + projected
    squares = lax.psum(jnp.sum(after_mixer * after_mixer, axis=1), "tp")
    normed_rows = (after_mixer * lax.rsqrt(squares / D + 1e-06)[:, None] * norm_gain).astype(
        jnp.bfloat16
    )
    full_rows = lax.all_gather(normed_rows, "tp", axis=1, tiled=True)
    gate_sum = jnp.dot(
        full_rows,
        lax.all_gather(gate_weight, "sp", axis=0, tiled=True),
        preferred_element_type=jnp.float32,
    )
    upward = jnp.dot(
        full_rows,
        lax.all_gather(up_weight, "sp", axis=0, tiled=True),
        preferred_element_type=jnp.float32,
    )
    gated = gate_sum.astype(jnp.bfloat16)
    padded = with_halo(gated, (("sp", 0),), 1).astype(jnp.float32)
    conv = (
        padded[:-2] * conv_weight[0]
        + padded[1:-1] * conv_weight[1]
        + padded[2:] * conv_weight[2]
        + conv_bias
    )
    hidden = (jax.nn.silu(conv) * upward).astype(jnp.bfloat16)
    partial_terms = jnp.dot(
        hidden,
        lax.all_gather(down_weight, "sp", axis=1, tiled=True),
        preferred_element_type=jnp.float32,
    )
    mixer_out = lax.psum_scatter(
        partial_terms.astype(jnp.bfloat16), "tp", scatter_dimension=1, tiled=True
    ).astype(jnp.float32)
    return (after_mixer + mixer_out).astype(jnp.bfloat16)


def solution(mesh):
    placed = (
        P("sp", "tp"),
        P("sp", "tp"),
        P("sp", "tp"),
        P("sp", "tp"),
        P("tp"),
        P(),
        P(None, "tp"),
        P("tp"),
        P("sp", "tp"),
        P("sp", "tp"),
        P(None, "tp"),
        P("tp"),
        P("tp", "sp"),
    )
    return jax.shard_map(
        on_device, mesh=mesh, in_specs=placed, out_specs=P("sp", "tp"), check_vma=False
    )
```

profile of v0, /device:TPU:0, one launch (start us, length us, event | category | flops | bytes accessed | tf_op | source)
XLA Modules:
  0.0 553.9 jit_solution(7031731348143616948)
XLA Ops:
  9.2 52.1 %all-gather.8.cloned.1.call-done = bf16[4096,256]{1,0:T(8,128)(2,1)} async-done(((bf16[512,256]{1,0:T(8,128)(2,1)}), bf16[4096,256]{1,0:T(8,128)(2,1)}) %all-gather.8.cloned.1.call-update) | async-done | bytes 2097168 | tf_op jit(solution)/shard_map/all_gather | solution.py:53
  61.3 8.3 %reshape.31 = bf16[2,2048,2,2,64]{4,3,2,1,0:T(2,128)(2,1)} reshape(bf16[4096,256]{1,0:T(8,128)(2,1)} %all-gather.8.cloned.1.call-done) | data formatting | bytes 4194304 | tf_op jit(solution)/shard_map/reshape | solution.py:57
  69.6 10.7 %copy.24 = bf16[2,2048,2,2,64]{1,4,3,2,0:T(8,128)(2,1)} copy(bf16[2,2048,2,2,64]{4,3,2,1,0:T(2,128)(2,1)} %reshape.31) | data formatting | bytes 4194304
  80.3 30.7 %all-gather.10.cloned.1.call-done = bf16[4096,256]{1,0:T(8,128)(2,1)} async-done(((bf16[512,256]{1,0:T(8,128)(2,1)}), bf16[4096,256]{1,0:T(8,128)(2,1)}) %all-gather.10.cloned.1.call-update) | async-done | bytes 2097168 | tf_op jit(solution)/shard_map/all_gather | solution.py:54
  111.1 4.0 reshape.29
  115.0 53.5 %while.15 = (s32[]{:T(128)}, f32[2,2,512]{2,1,0:T(2,128)S(1)}, f32[2,2,512]{2,1,0:T(2,128)S(1)}, f32[2,2,512,128]{3,2,1,0:T(8,128)S(1)}, bf16[2,2048,2,2,64]{1,4...) while((s32[]{:T(128)}, f32[2,2,512]{2,1,0:T(2,128)S(1)}, ...), condition=%wide.region_3.4_spmd.clone, body=%wide.region_0.3_spmd.clone.sunk | while | flops 1644963840 | bytes 65405572 | solution.py:81
  115.0 9.3 %bitcast_reduce_fusion.2 = (f32[2,2,512]{2,1,0:T(2,128)S(1)}, f32[2,2,2048,512]{3,2,1,0:T(8,128)}) fusion(bf16[512,2,2,64]{0,3,2,1:T(8,128)(2,1)S(1)} %get-tuple-element.175, bf16[2,2048,2,2,64]{1,4,3,2,0:T(8,128)(2,1)} %get-tuple-element.174, s32[]{:T(128)} %get-tuple-element.161), kind=kOutput, calls=%fused_computation.1.clone.1 | convolution fusion | flops 545257472 | bytes 18096640 | tf_op jit(solution)/shard_map/while/body/eval_jaxpr/qhmd,khmd->hmqk/dot_general | solution.py:64
  124.4 8.6 %fusion.40 = f32[2,2,512]{2,1,0:T(2,128)S(1)} fusion(f32[2,2,2048,512]{3,2,1,0:T(8,128)} %get-tuple-element.149, f32[2,2,512]{2,1,0:T(2,128)S(1)} %fusion.39), kind=kLoop, calls=%fused_computation.4.clone.1 | loop fusion | flops 12580864 | bytes 16793600 | tf_op jit(solution)/shard_map/while/body/eval_jaxpr/reduce_sum | solution.py:72
  133.9 7.9 %fusion.42 = f32[2,2,512,128]{3,2,1,0:T(8,128)S(1)} fusion(f32[2,2,2048,512]{3,2,1,0:T(8,128)} %get-tuple-element.149, f32[2,2,512]{2,1,0:T(2,128)S(1)} %fusion.39, bf16[1,2048,2,128]{3,2,1,0:T(2,128)(2,1)S(1)} %constant_dynamic-slice_fusion.2, f32[2,2,512,128]{3,2,1,0:T(8,128)S(1)} %get-tuple-element.164, f32[2,2,512]{2,1,0:T(2,128)S(1)} %get-tuple-element.151, ...), kind=kOutput, calls=%fused_computation.6.clone.1 | convolution fusion | flops 1087111168 | bytes 19939328 | tf_op jit(solution)/shard_map/while/body/eval_jaxpr/hmqk,khe->hmqe/dot_general | solution.py:73
  141.8 9.3 %bitcast_reduce_fusion.2 = (f32[2,2,512]{2,1,0:T(2,128)S(1)}, f32[2,2,2048,512]{3,2,1,0:T(8,128)}) fusion(bf16[512,2,2,64]{0,3,2,1:T(8,128)(2,1)S(1)} %get-tuple-element.175, bf16[2,2048,2,2,64]{1,4,3,2,0:T(8,128)(2,1)} %get-tuple-element.174, s32[]{:T(128)} %get-tuple-element.161), kind=kOutput, calls=%fused_computation.1.clone.1 | convolution fusion | flops 545257472 | bytes 18096640 | tf_op jit(solution)/shard_map/while/body/eval_jaxpr/qhmd,khmd->hmqk/dot_general | solution.py:64
  151.2 8.6 %fusion.40 = f32[2,2,512]{2,1,0:T(2,128)S(1)} fusion(f32[2,2,2048,512]{3,2,1,0:T(8,128)} %get-tuple-element.149, f32[2,2,512]{2,1,0:T(2,128)S(1)} %fusion.39), kind=kLoop, calls=%fused_computation.4.clone.1 | loop fusion | flops 12580864 | bytes 16793600 | tf_op jit(solution)/shard_map/while/body/eval_jaxpr/reduce_sum | solution.py:72
  160.6 7.9 %fusion.42 = f32[2,2,512,128]{3,2,1,0:T(8,128)S(1)} fusion(f32[2,2,2048,512]{3,2,1,0:T(8,128)} %get-tuple-element.149, f32[2,2,512]{2,1,0:T(2,128)S(1)} %fusion.39, bf16[1,2048,2,128]{3,2,1,0:T(2,128)(2,1)S(1)} %constant_dynamic-slice_fusion.2, f32[2,2,512,128]{3,2,1,0:T(8,128)S(1)} %get-tuple-element.164, f32[2,2,512]{2,1,0:T(2,128)S(1)} %get-tuple-element.151, ...), kind=kOutput, calls=%fused_computation.6.clone.1 | convolution fusion | flops 1087111168 | bytes 19939328 | tf_op jit(solution)/shard_map/while/body/eval_jaxpr/hmqk,khe->hmqe/dot_general | solution.py:73
  170.8 14.9 %all-gather.12.cloned.1.call-done = bf16[512,1024]{0,1:T(8,128)(2,1)} async-done(((bf16[512,256]{0,1:T(8,128)(2,1)}), bf16[512,1024]{0,1:T(8,128)(2,1)}) %all-gather.12.cloned.1.call-update) | async-done | bytes 1048592 | tf_op jit(solution)/shard_map/all_gather | solution.py:89
  185.7 2.0 multiply_reduce_fusion
  187.7 5.9 %psum.7 = f32[512]{0:T(512)S(1)} all-reduce(f32[512]{0:T(512)S(1)} %get-tuple-element.99), channel_id=1, replica_groups=mesh['sp'=8,'tp'=4] {'tp'}, use_global_device_ids=true, to_apply=%region_6.7 | all-reduce | flops 512 | bytes 4096 | tf_op jit(solution)/shard_map/psum | solution.py:94
  196.5 21.8 %all-gather.14.cloned.1.call-done = bf16[512,2048]{0,1:T(8,128)(2,1)} async-done(((bf16[512,512]{0,1:T(8,128)(2,1)}), bf16[512,2048]{0,1:T(8,128)(2,1)}) %all-gather.14.cloned.1.call-update) | async-done | bytes 2097168 | tf_op jit(solution)/shard_map/all_gather | solution.py:98
  218.3 94.4 %all-gather.16.cloned.1.call-done = bf16[2048,1408]{1,0:T(8,128)(2,1)} async-done(((bf16[256,1408]{1,0:T(8,128)(2,1)}), bf16[2048,1408]{1,0:T(8,128)(2,1)}) %all-gather.16.cloned.1.call-update) | async-done | bytes 5767184 | tf_op jit(solution)/shard_map/all_gather | solution.py:101
  312.7 6.7 %convolution_convert_fusion = bf16[512,1408]{1,0:T(8,128)(2,1)S(1)} fusion(bf16[512,2048]{0,1:T(8,128)(2,1)} %all-gather.14.cloned.1.call-done, bf16[2048,1408]{1,0:T(8,128)(2,1)} %all-gather.16.cloned.1.call-done), kind=kOutput, calls=%fused_computation.22 | convolution fusion | flops 2953510912 | bytes 9306112 | tf_op jit(solution)/shard_map/dot_general | solution.py:99
  319.5 2.5 collective-permute-start
  323.3 4.4 collective-permute-done.1
  329.7 75.6 %all-gather.18.cloned.1.call-done = bf16[2048,1408]{1,0:T(8,128)(2,1)} async-done(((bf16[256,1408]{1,0:T(8,128)(2,1)}), bf16[2048,1408]{1,0:T(8,128)(2,1)}) %all-gather.18.cloned.1.call-update) | async-done | bytes 5767184 | tf_op jit(solution)/shard_map/all_gather | solution.py:106
  405.3 93.4 %all-gather.20.cloned.1.call-done = bf16[1408,2048]{1,0:T(8,128)(2,1)} async-done(((bf16[1408,256]{1,0:T(8,128)(2,1)}), bf16[1408,2048]{1,0:T(8,128)(2,1)}) %all-gather.20.cloned.1.call-update) | async-done | bytes 5767184 | tf_op jit(solution)/shard_map/all_gather | solution.py:120
  498.7 16.7 %convolution_convert_fusion.1 = bf16[512,2048]{0,1:T(8,128)(2,1)} fusion(bf16[1408,2048]{1,0:T(8,128)(2,1)} %all-gather.20.cloned.1.call-done, bf16[512,2048]{0,1:T(8,128)(2,1)} %all-gather.14.cloned.1.call-done, bf16[2048,1408]{1,0:T(8,128)(2,1)} %all-gather.18.cloned.1.call-done, f32[514,1408]{1,0:T(8,128)} %maximum_convert_fusion, ...), kind=kOutput, calls=%fused_computation.23 | convolution fusion | flops 5915279360 | bytes 24401920 | tf_op jit(solution)/shard_map/dot_general | solution.py:118
  515.4 29.5 %reduce-scatter.2.cloned.1.call-done = bf16[512,512]{0,1:T(8,128)(2,1)} async-done(((bf16[512,2048]{0,1:T(8,128)(2,1)}), bf16[512,512]{0,1:T(8,128)(2,1)}) %reduce-scatter.2.cloned.1.call-update) | async-done | bytes 524304 | tf_op jit(solution)/shard_map/reduce_scatter | solution.py:123
  (62 shorter events, 14.8 us)
Async XLA Ops:
  6.5 179.2 %copy-start = (bf16[1024,512]{1,0:T(8,128)(2,1)S(1)}, bf16[1024,512]{1,0:T(8,128)(2,1)}, u32[]{:S(2)}) copy-start(bf16[1024,512]{1,0:T(8,128)(2,1)} %param.21) | copy-start | bytes 3145732
  6.5 54.8 %all-gather.8.cloned.1.call-start = ((), (), s32[]{:S(2)}) async-start(), calls=%async_computation.1 | async-start | bytes 2359296 | tf_op jit(solution)/shard_map/all_gather | solution.py:53
  7.3 103.8 %all-gather.10.cloned.1.call-start = ((), (), s32[]{:S(2)}) async-start(), calls=%async_computation.2 | async-start | bytes 2359296 | tf_op jit(solution)/shard_map/all_gather | solution.py:54
  8.0 177.7 %all-gather.12.cloned.1.call-start = ((), (), s32[]{:S(2)}) async-start(), calls=%async_computation.3 | async-start | bytes 1310720 | tf_op jit(solution)/shard_map/all_gather | solution.py:89
  124.4 8.7 %copy-start.1 = (bf16[2,2048,2,128]{3,2,1,0:T(2,128)(2,1)S(1)}, bf16[2,2048,2,128]{3,2,1,0:T(2,128)(2,1)}, u32[]{:S(2)}) copy-start(bf16[2,2048,2,128]{3,2,1,0:T(2,128)(2,1)} %get-tuple-element.176) | copy-start | bytes 6291460 | tf_op jit(solution)/shard_map/while
  151.1 8.7 %copy-start.1 = (bf16[2,2048,2,128]{3,2,1,0:T(2,128)(2,1)S(1)}, bf16[2,2048,2,128]{3,2,1,0:T(2,128)(2,1)}, u32[]{:S(2)}) copy-start(bf16[2,2048,2,128]{3,2,1,0:T(2,128)(2,1)} %get-tuple-element.176) | copy-start | bytes 6291460 | tf_op jit(solution)/shard_map/while
  168.5 0.7 copy-start.5
  168.6 0.8 copy-start.6
  168.9 1.6 copy-start.2
  170.3 48.0 %all-gather.14.cloned.1.call-start = ((), (), s32[]{:S(2)}) async-start(), calls=%async_computation.4 | async-start | bytes 2621440 | tf_op jit(solution)/shard_map/all_gather | solution.py:98
  170.8 22.8 %copy-start.4 = (f32[512]{0:T(512)S(1)}, f32[512]{0:T(512)}, u32[]{:S(2)}) copy-start(f32[512]{0:T(512)} %param.22) | copy-start | bytes 6148
  194.6 118.2 %all-gather.16.cloned.1.call-start = ((), (), s32[]{:S(2)}) async-start(), calls=%async_computation.5 | async-start | bytes 6488064 | tf_op jit(solution)/shard_map/all_gather | solution.py:101
  195.1 210.1 %all-gather.18.cloned.1.call-start = ((), (), s32[]{:S(2)}) async-start(), calls=%async_computation.6 | async-start | bytes 6488064 | tf_op jit(solution)/shard_map/all_gather | solution.py:106
  195.7 302.9 %all-gather.20.cloned.1.call-start = ((), (), s32[]{:S(2)}) async-start(), calls=%async_computation.7 | async-start | bytes 6488064 | tf_op jit(solution)/shard_map/all_gather | solution.py:120
  196.5 126.8 %copy-start.3 = (f32[3,1408]{1,0:T(4,128)S(1)}, f32[3,1408]{1,0:T(4,128)}, u32[]{:S(2)}) copy-start(f32[3,1408]{1,0:T(4,128)} %param.25) | copy-start | bytes 50692
  196.5 348.4 %reduce-scatter.2.cloned.1.call-start = ((), (), s32[]{:S(2)}) async-start(), calls=%async_computation.8 | async-start | bytes 2621440 | tf_op jit(solution)/shard_map/reduce_scatter | solution.py:123
  319.4 179.2 %copy-start.7 = (f32[1408]{0:T(1024)S(1)}, f32[1408]{0:T(1024)}, u32[]{:S(2)}) copy-start(f32[1408]{0:T(1024)} %param.26) | copy-start | bytes 16900
  319.5 3.8 collective-permute-start
  321.9 5.8 %collective-permute-start.1 = (bf16[1,1408]{1,0:T(2,128)(2,1)S(1)}, bf16[1,1408]{1,0:T(2,128)(2,1)S(1)}, u32[]{:S(2)}, u32[]{:S(2)}) collective-permute-start(bf16[1,1408]{1,0:T(2,128)(2,1)S(1)} %get-tuple-element.98), channel_id=1, source_target_pairs={{4,0},{8,4},{12,8},{16,12},{20,16},{24,20},{28,24},{5,1},{9,5},{13... | collective-permute-start | bytes 8456 | tf_op jit(solution)/shard_map/ppermute | solution.py:22
Sparse Core Ops, SparseCore 0:
  9.5 51.7 all-gather.7
  63.4 47.6 all-gather.9
  170.4 15.2 all-gather.11
  194.7 23.6 all-gather.13
  220.4 92.3 all-gather.15
  314.7 90.4 all-gather.17
  407.3 91.2 all-gather.19
  515.5 29.3 reduce-scatter.1
where the time goes:
time: 555 us; the launch traced here: 554 us
  waiting for transfers between devices  420 us (76%)
  matrix products  59.9 us (11%)
  local copies, waits for them, and re-layouts  27.4 us (5%)
  other arithmetic  22.7 us (4%)
  between operations  13.7 us (2%)
  blocking collectives  5.88 us (1%)
    all_gather x1, waiting for transfers between devices, on_device(): lax.all_gather(gate_weight, 'sp', axis=0, tiled=True)  94.4 us
    all_gather x1, waiting for transfers between devices, on_device(): lax.all_gather(down_weight, 'sp', axis=1, tiled=True)  93.4 us
    all_gather x1, waiting for transfers between devices, on_device(): lax.all_gather(up_weight, 'sp', axis=0, tiled=True)  75.6 us
    all_gather x1, waiting for transfers between devices, on_device(): key_rows = lax.all_gather(keys, 'sp', axis=0, tiled=True)  52.1 us
    all_gather x1, waiting for transfers between devices, on_device(): value_rows = lax.all_gather(values, 'sp', axis=0, tiled=True)  30.7 us
    reduce_scatter x1, waiting for transfers between devices, on_device(): lax.psum_scatter(partial_terms.astype(jnp.bfloat16), 'tp', scatter_dimens...  29.5 us
    all_gather x1, waiting for transfers between devices, on_device(): full_rows = lax.all_gather(normed_rows, 'tp', axis=1, tiled=True)  21.8 us
    dot_general x2, matrix products, advance(): jnp.einsum('qhmd,khmd->hmqk', query_heads, key_block, preferred_element_t...  18.7 us
  transfers between devices with their start and end apart: 10, of which 9 were waited for; matrix products, arithmetic and copies ran while one was open for 5% of the time, Pallas kernels for 0%

commit v1 on v0

--- a/solution.py
+++ b/solution.py
@@ -117,7 +117,7 @@
     hidden = (jax.nn.silu(conv) * upward).astype(jnp.bfloat16)
     partial_terms = jnp.dot(
         hidden,
-        lax.all_gather(down_weight, "sp", axis=1, tiled=True),
+        jnp.concatenate(lax.all_gather(down_weight, "sp"), axis=1),
         preferred_element_type=jnp.float32,
     )
     mixer_out = lax.psum_scatter(

time: 555 us -> 554 us (level)
  waiting for transfers between devices: 420 us -> 408 us
  local copies, waits for them, and re-layouts: 27.4 us -> 37.7 us
    all_gather x1, waiting for transfers between devices: 93.4 us -> 79.5 us  [on_device(): lax.all_gather(down_weight, 'sp')]
    reshape x0 -> x1, local copies, waits for them, and re-layouts: none -> 8.29 us  [on_device(): jnp.concatenate(lax.all_gather(down_weight, 'sp'), axis=1)]
    all_gather x1, waiting for transfers between devices: 75.6 us -> 81.7 us  [on_device(): lax.all_gather(up_weight, 'sp', axis=0, tiled=True)]
    unnamed x17 -> x13, local copies, waits for them, and re-layouts: 12.2 us -> 12.1 us
  transfers between devices with their start and end apart: 10 -> 10, of which waited for: 9 -> 8; matrix products, arithmetic and copies ran while one was open for 5% -> 7% of each run, Pallas kernels for 0% -> 0%
where the time goes in v1:
time: 554 us; the launch traced here: 553 us
  waiting for transfers between devices  408 us (74%)
  matrix products  59.7 us (11%)
  local copies, waits for them, and re-layouts  37.7 us (7%)
  other arithmetic  23.4 us (4%)
  between operations  13.6 us (2%)
  blocking collectives  5.88 us (1%)
    all_gather x1, waiting for transfers between devices, on_device(): lax.all_gather(gate_weight, 'sp', axis=0, tiled=True)  94.4 us
    all_gather x1, waiting for transfers between devices, on_device(): lax.all_gather(up_weight, 'sp', axis=0, tiled=True)  81.7 us
    all_gather x1, waiting for transfers between devices, on_device(): lax.all_gather(down_weight, 'sp')  79.5 us
    all_gather x1, waiting for transfers between devices, on_device(): key_rows = lax.all_gather(keys, 'sp', axis=0, tiled=True)  52.1 us
    all_gather x1, waiting for transfers between devices, on_device(): value_rows = lax.all_gather(values, 'sp', axis=0, tiled=True)  30.8 us
    reduce_scatter x1, waiting for transfers between devices, on_device(): lax.psum_scatter(partial_terms.astype(jnp.bfloat16), 'tp', scatter_dimens...  29.5 us
    all_gather x1, waiting for transfers between devices, on_device(): full_rows = lax.all_gather(normed_rows, 'tp', axis=1, tiled=True)  21.8 us
    dot_general x2, matrix products, advance(): jnp.einsum('qhmd,khmd->hmqk', query_heads, key_block, preferred_element_t...  18.7 us
  transfers between devices with their start and end apart: 10, of which 8 were waited for; matrix products, arithmetic and copies ran while one was open for 7% of the time, Pallas kernels for 0%

profile of v1, /device:TPU:0, one launch (start us, length us, event | category | flops | bytes accessed | tf_op | source)
XLA Modules:
  0.0 553.1 jit_solution(7220179585889094106)
XLA Ops:
  9.2 52.1 %all-gather.9.cloned.1.call-done = bf16[4096,256]{1,0:T(8,128)(2,1)} async-done(((bf16[512,256]{1,0:T(8,128)(2,1)}), bf16[4096,256]{1,0:T(8,128)(2,1)}) %all-gather.9.cloned.1.call-update) | async-done | bytes 2097168 | tf_op jit(solution)/shard_map/all_gather | solution.py:53
  61.3 8.3 %reshape.40 = bf16[2,2048,2,2,64]{4,3,2,1,0:T(2,128)(2,1)} reshape(bf16[4096,256]{1,0:T(8,128)(2,1)} %all-gather.9.cloned.1.call-done) | data formatting | bytes 4194304 | tf_op jit(solution)/shard_map/reshape | solution.py:57
  69.6 10.7 %copy.34 = bf16[2,2048,2,2,64]{1,4,3,2,0:T(8,128)(2,1)} copy(bf16[2,2048,2,2,64]{4,3,2,1,0:T(2,128)(2,1)} %reshape.40) | data formatting | bytes 4194304
  80.3 30.8 %all-gather.11.cloned.1.call-done = bf16[4096,256]{1,0:T(8,128)(2,1)} async-done(((bf16[512,256]{1,0:T(8,128)(2,1)}), bf16[4096,256]{1,0:T(8,128)(2,1)}) %all-gather.11.cloned.1.call-update) | async-done | bytes 2097168 | tf_op jit(solution)/shard_map/all_gather | solution.py:54
  111.1 4.0 reshape.35
  115.0 53.5 %while.15 = (s32[]{:T(128)}, f32[2,2,512]{2,1,0:T(2,128)S(1)}, f32[2,2,512]{2,1,0:T(2,128)S(1)}, f32[2,2,512,128]{3,2,1,0:T(8,128)S(1)}, bf16[2,2048,2,2,64]{1,4...) while((s32[]{:T(128)}, f32[2,2,512]{2,1,0:T(2,128)S(1)}, ...), condition=%wide.region_3.4_spmd.clone, body=%wide.region_0.3_spmd.clone.sunk | while | flops 1644963840 | bytes 65405572 | solution.py:81
  115.0 9.3 %bitcast_reduce_fusion.2 = (f32[2,2,512]{2,1,0:T(2,128)S(1)}, f32[2,2,2048,512]{3,2,1,0:T(8,128)}) fusion(bf16[512,2,2,64]{0,3,2,1:T(8,128)(2,1)S(1)} %get-tuple-element.182, bf16[2,2048,2,2,64]{1,4,3,2,0:T(8,128)(2,1)} %get-tuple-element.181, s32[]{:T(128)} %get-tuple-element.168), kind=kOutput, calls=%fused_computation.1.clone.1 | convolution fusion | flops 545257472 | bytes 18096640 | tf_op jit(solution)/shard_map/while/body/eval_jaxpr/qhmd,khmd->hmqk/dot_general | solution.py:64
  124.4 8.6 %fusion.40 = f32[2,2,512]{2,1,0:T(2,128)S(1)} fusion(f32[2,2,2048,512]{3,2,1,0:T(8,128)} %get-tuple-element.156, f32[2,2,512]{2,1,0:T(2,128)S(1)} %fusion.39), kind=kLoop, calls=%fused_computation.4.clone.1 | loop fusion | flops 12580864 | bytes 16793600 | tf_op jit(solution)/shard_map/while/body/eval_jaxpr/reduce_sum | solution.py:72
  133.9 7.9 %fusion.42 = f32[2,2,512,128]{3,2,1,0:T(8,128)S(1)} fusion(f32[2,2,2048,512]{3,2,1,0:T(8,128)} %get-tuple-element.156, f32[2,2,512]{2,1,0:T(2,128)S(1)} %fusion.39, bf16[1,2048,2,128]{3,2,1,0:T(2,128)(2,1)S(1)} %constant_dynamic-slice_fusion.2, f32[2,2,512,128]{3,2,1,0:T(8,128)S(1)} %get-tuple-element.171, f32[2,2,512]{2,1,0:T(2,128)S(1)} %get-tuple-element.158, ...), kind=kOutput, calls=%fused_computation.6.clone.1 | convolution fusion | flops 1087111168 | bytes 19939328 | tf_op jit(solution)/shard_map/while/body/eval_jaxpr/hmqk,khe->hmqe/dot_general | solution.py:73
  141.8 9.4 %bitcast_reduce_fusion.2 = (f32[2,2,512]{2,1,0:T(2,128)S(1)}, f32[2,2,2048,512]{3,2,1,0:T(8,128)}) fusion(bf16[512,2,2,64]{0,3,2,1:T(8,128)(2,1)S(1)} %get-tuple-element.182, bf16[2,2048,2,2,64]{1,4,3,2,0:T(8,128)(2,1)} %get-tuple-element.181, s32[]{:T(128)} %get-tuple-element.168), kind=kOutput, calls=%fused_computation.1.clone.1 | convolution fusion | flops 545257472 | bytes 18096640 | tf_op jit(solution)/shard_map/while/body/eval_jaxpr/qhmd,khmd->hmqk/dot_general | solution.py:64
  151.2 8.6 %fusion.40 = f32[2,2,512]{2,1,0:T(2,128)S(1)} fusion(f32[2,2,2048,512]{3,2,1,0:T(8,128)} %get-tuple-element.156, f32[2,2,512]{2,1,0:T(2,128)S(1)} %fusion.39), kind=kLoop, calls=%fused_computation.4.clone.1 | loop fusion | flops 12580864 | bytes 16793600 | tf_op jit(solution)/shard_map/while/body/eval_jaxpr/reduce_sum | solution.py:72
  160.6 7.9 %fusion.42 = f32[2,2,512,128]{3,2,1,0:T(8,128)S(1)} fusion(f32[2,2,2048,512]{3,2,1,0:T(8,128)} %get-tuple-element.156, f32[2,2,512]{2,1,0:T(2,128)S(1)} %fusion.39, bf16[1,2048,2,128]{3,2,1,0:T(2,128)(2,1)S(1)} %constant_dynamic-slice_fusion.2, f32[2,2,512,128]{3,2,1,0:T(8,128)S(1)} %get-tuple-element.171, f32[2,2,512]{2,1,0:T(2,128)S(1)} %get-tuple-element.158, ...), kind=kOutput, calls=%fused_computation.6.clone.1 | convolution fusion | flops 1087111168 | bytes 19939328 | tf_op jit(solution)/shard_map/while/body/eval_jaxpr/hmqk,khe->hmqe/dot_general | solution.py:73
  170.8 14.9 %all-gather.13.cloned.1.call-done = bf16[512,1024]{0,1:T(8,128)(2,1)} async-done(((bf16[512,256]{0,1:T(8,128)(2,1)}), bf16[512,1024]{0,1:T(8,128)(2,1)}) %all-gather.13.cloned.1.call-update) | async-done | bytes 1048592 | tf_op jit(solution)/shard_map/all_gather | solution.py:89
  187.7 5.9 %psum.7 = f32[512]{0:T(512)S(1)} all-reduce(f32[512]{0:T(512)S(1)} %get-tuple-element.106), channel_id=1, replica_groups=mesh['sp'=8,'tp'=4] {'tp'}, use_global_device_ids=true, to_apply=%region_6.7 | all-reduce | flops 512 | bytes 4096 | tf_op jit(solution)/shard_map/psum | solution.py:94
  196.5 21.8 %all-gather.15.cloned.1.call-done = bf16[512,2048]{0,1:T(8,128)(2,1)} async-done(((bf16[512,512]{0,1:T(8,128)(2,1)}), bf16[512,2048]{0,1:T(8,128)(2,1)}) %all-gather.15.cloned.1.call-update) | async-done | bytes 2097168 | tf_op jit(solution)/shard_map/all_gather | solution.py:98
  218.4 94.4 %all-gather.17.cloned.1.call-done = bf16[2048,1408]{1,0:T(8,128)(2,1)} async-done(((bf16[256,1408]{1,0:T(8,128)(2,1)}), bf16[2048,1408]{1,0:T(8,128)(2,1)}) %all-gather.17.cloned.1.call-update) | async-done | bytes 5767184 | tf_op jit(solution)/shard_map/all_gather | solution.py:101
  312.7 6.7 %convolution_convert_fusion = bf16[512,1408]{1,0:T(8,128)(2,1)S(1)} fusion(bf16[512,2048]{0,1:T(8,128)(2,1)} %all-gather.15.cloned.1.call-done, bf16[2048,1408]{1,0:T(8,128)(2,1)} %all-gather.17.cloned.1.call-done), kind=kOutput, calls=%fused_computation.22 | convolution fusion | flops 2953510912 | bytes 9306112 | tf_op jit(solution)/shard_map/dot_general | solution.py:99
  320.1 3.0 collective-permute-start
  325.9 79.5 %all-gather.21.cloned.1.call-done = bf16[11264,256]{1,0:T(8,128)(2,1)} async-done(((bf16[1408,256]{1,0:T(8,128)(2,1)}), bf16[11264,256]{1,0:T(8,128)(2,1)}) %all-gather.21.cloned.1.call-update) | async-done | bytes 5767184 | tf_op jit(solution)/shard_map/all_gather | solution.py:120
  405.3 8.3 %copy.38 = bf16[1408,8,256]{0,2,1:T(8,128)(2,1)} copy(bf16[1408,8,256]{2,0,1:T(8,128)(2,1)} %bitcast.70) | data formatting | bytes 11534336 | tf_op jit(solution)/shard_map/reshape | solution.py:120
  413.6 2.7 maximum_convert_fusion
  416.3 81.7 %all-gather.19.cloned.1.call-done = bf16[2048,1408]{1,0:T(8,128)(2,1)} async-done(((bf16[256,1408]{1,0:T(8,128)(2,1)}), bf16[2048,1408]{1,0:T(8,128)(2,1)}) %all-gather.19.cloned.1.call-update) | async-done | bytes 5767184 | tf_op jit(solution)/shard_map/all_gather | solution.py:106
  498.0 16.5 %convolution_convert_fusion.1 = bf16[512,2048]{0,1:T(8,128)(2,1)} fusion(bf16[1408,2048]{0,1:T(8,128)(2,1)} %bitcast.71, bf16[512,2048]{0,1:T(8,128)(2,1)} %all-gather.15.cloned.1.call-done, bf16[2048,1408]{1,0:T(8,128)(2,1)} %all-gather.19.cloned.1.call-done, f32[514,1408]{1,0:T(8,128)} %maximum_convert_fusion, f32[1408]{0:T(1024)} %param.26, ...), kind=kOutput, calls=%fused_computation.23 | convolution fusion | flops 5915279360 | bytes 24407040 | tf_op jit(solution)/shard_map/dot_general | solution.py:118
  514.6 29.5 %reduce-scatter.2.cloned.1.call-done = bf16[512,512]{0,1:T(8,128)(2,1)} async-done(((bf16[512,2048]{0,1:T(8,128)(2,1)}), bf16[512,512]{0,1:T(8,128)(2,1)}) %reduce-scatter.2.cloned.1.call-update) | async-done | bytes 524304 | tf_op jit(solution)/shard_map/reduce_scatter | solution.py:123
  (59 shorter events, 16.8 us)
Async XLA Ops:
  6.5 179.2 %copy-start = (bf16[1024,512]{1,0:T(8,128)(2,1)S(1)}, bf16[1024,512]{1,0:T(8,128)(2,1)}, u32[]{:S(2)}) copy-start(bf16[1024,512]{1,0:T(8,128)(2,1)} %param.21) | copy-start | bytes 3145732
  6.5 54.8 %all-gather.9.cloned.1.call-start = ((), (), s32[]{:S(2)}) async-start(), calls=%async_computation.1 | async-start | bytes 2359296 | tf_op jit(solution)/shard_map/all_gather | solution.py:53
  7.3 103.8 %all-gather.11.cloned.1.call-start = ((), (), s32[]{:S(2)}) async-start(), calls=%async_computation.2 | async-start | bytes 2359296 | tf_op jit(solution)/shard_map/all_gather | solution.py:54
  8.0 177.7 %all-gather.13.cloned.1.call-start = ((), (), s32[]{:S(2)}) async-start(), calls=%async_computation.3 | async-start | bytes 1310720 | tf_op jit(solution)/shard_map/all_gather | solution.py:89
  124.4 8.7 %copy-start.1 = (bf16[2,2048,2,128]{3,2,1,0:T(2,128)(2,1)S(1)}, bf16[2,2048,2,128]{3,2,1,0:T(2,128)(2,1)}, u32[]{:S(2)}) copy-start(bf16[2,2048,2,128]{3,2,1,0:T(2,128)(2,1)} %get-tuple-element.183) | copy-start | bytes 6291460 | tf_op jit(solution)/shard_map/while
  151.2 8.7 %copy-start.1 = (bf16[2,2048,2,128]{3,2,1,0:T(2,128)(2,1)S(1)}, bf16[2,2048,2,128]{3,2,1,0:T(2,128)(2,1)}, u32[]{:S(2)}) copy-start(bf16[2,2048,2,128]{3,2,1,0:T(2,128)(2,1)} %get-tuple-element.183) | copy-start | bytes 6291460 | tf_op jit(solution)/shard_map/while
  168.6 0.7 copy-start.4
  168.6 0.8 copy-start.5
  168.9 1.6 copy-start.2
  170.3 48.0 %all-gather.15.cloned.1.call-start = ((), (), s32[]{:S(2)}) async-start(), calls=%async_computation.4 | async-start | bytes 2621440 | tf_op jit(solution)/shard_map/all_gather | solution.py:98
  170.8 22.8 %copy-start.3 = (f32[512]{0:T(512)S(1)}, f32[512]{0:T(512)}, u32[]{:S(2)}) copy-start(f32[512]{0:T(512)} %param.22) | copy-start | bytes 6148
  194.6 118.2 %all-gather.17.cloned.1.call-start = ((), (), s32[]{:S(2)}) async-start(), calls=%async_computation.5 | async-start | bytes 6488064 | tf_op jit(solution)/shard_map/all_gather | solution.py:101
  195.2 210.2 %all-gather.21.cloned.1.call-start = ((), (), s32[]{:S(2)}) async-start(), calls=%async_computation.8 | async-start | bytes 6488064 | tf_op jit(solution)/shard_map/all_gather | solution.py:120
  195.7 302.3 %all-gather.19.cloned.1.call-start = ((), (), s32[]{:S(2)}) async-start(), calls=%async_computation.6 | async-start | bytes 6488064 | tf_op jit(solution)/shard_map/all_gather | solution.py:106
  196.5 347.6 %reduce-scatter.2.cloned.1.call-start = ((), (), s32[]{:S(2)}) async-start(), calls=%async_computation.7 | async-start | bytes 2621440 | tf_op jit(solution)/shard_map/reduce_scatter | solution.py:123
  320.1 93.6 %collective-permute-start = (bf16[1,1408]{1,0:T(2,128)(2,1)}, bf16[1,1408]{1,0:T(2,128)(2,1)}, u32[]{:S(2)}, u32[]{:S(2)}) collective-permute-start(bf16[1,1408]{1,0:T(2,128)(2,1)} %get-tuple-element.104), channel_id=1, source_target_pairs={{0,4},{4,8},{8,12},{12,16},{16,20},{20,24},{24,28},{1,5},{5,9},{9,... | collective-permute-start | bytes 8456 | tf_op jit(solution)/shard_map/ppermute | solution.py:20
  323.1 90.5 %collective-permute-start.1 = (bf16[1,1408]{1,0:T(2,128)(2,1)}, bf16[1,1408]{1,0:T(2,128)(2,1)}, u32[]{:S(2)}, u32[]{:S(2)}) collective-permute-start(bf16[1,1408]{1,0:T(2,128)(2,1)} %get-tuple-element.105), channel_id=1, source_target_pairs={{4,0},{8,4},{12,8},{16,12},{20,16},{24,20},{28,24},{5,1},{9,5},{13... | collective-permute-start | bytes 8456 | tf_op jit(solution)/shard_map/ppermute | solution.py:22
Sparse Core Ops, SparseCore 0:
  9.5 51.7 all-gather.8
  63.4 47.6 all-gather.10
  170.4 15.2 all-gather.12
  194.7 23.6 all-gather.14
  220.4 92.3 all-gather.16
  314.8 90.5 all-gather.20
  407.5 90.4 all-gather.18
  514.7 29.3 reduce-scatter.1
